TPU v7x, 128 devices: a whole 4x4x4 slice. The times are simulated.
128 devices in a mesh: ep: 32 (over z, y, core), tp: 4 (over x).
Axes of the slice: x: 4, y: 4, z: 4, core: 2. Of those that a mesh axis runs over, the one named last changes fastest.
Arguments:
- queries: bfloat16 [32768, 1024], P('ep', 'tp'), may hold values from -6 to 6
- key_rows: bfloat16 [32768, 256], P('ep', 'tp'), may hold values from -6 to 6
- values: bfloat16 [32768, 256], P('ep', 'tp'), may hold values from -6 to 6
- sink_logit: float32 [16], P('tp'), may hold values from 3 to 7
- out_weight: bfloat16 [1024, 2048], P('tp'), may hold values from -0.1875 to 0.1875
- out_gain: float32 [2048], replicated, may hold values from 0.1 to 1.9
- routed_tokens: bfloat16 [65536, 2048], P(('ep', 'tp')), may hold values from -6 to 6
- expert_ids: int32 [65536, 2], P(('ep', 'tp')), may hold values from 0 to 31, as said below
- route_weight: float32 [65536, 2], P(('ep', 'tp')), may hold values from 0.1 to 1
- routed_gain: float32 [2048], replicated, may hold values from 0.1 to 1.9
- expert_gate: bfloat16 [32, 2048, 1024], P('ep', None, 'tp'), may hold values from -0.125 to 0.125
- expert_up: bfloat16 [32, 2048, 1024], P('ep', None, 'tp'), may hold values from -0.125 to 0.125
- expert_down: bfloat16 [32, 2048, 1024], P('ep', None, 'tp'), may hold values from -0.1875 to 0.1875
Outputs:
- mixer_out: bfloat16 [32768, 2048], P(('ep', 'tp'))
- experts_out: bfloat16 [65536, 2048], P(('ep', 'tp'))
Inputs may be any that keep to these rules, and one draw needn't show every extreme that they name: `expert_ids`: both experts of a row lie in one group (equal id // 8); the 512 rows of one device name every group exactly 512 / 4 times; the rows of one device name no expert more than 64 times; in every device's rows some expert of each group is named exactly 64 times, and one expert is named exactly 64 times by the rows of every device.
All inputs are finite; a program needn't handle non-finite values.
Results may differ from a plain program's by a relative error of at most 0.0071.
Values may be sent and summed in bfloat16 or wider, within the bound.
A program may use at most 128 MiB of HBM per device.

v0:
```python
import jax
import jax.numpy as jnp
from jax import lax
from jax.sharding import PartitionSpec as P

HEAD_DIM = 64
WINDOW = 128
QBLOCK = 512
EXPERTS = 32
TOP = 2
CAP = 64


epsilon = 1e-06


def padded(block, sides, width):
    for axis, dim in sides:
        count = lax.axis_size(axis)
        forward = [(i, i + 1) for i in range(count - 1)]
        backward = [(target, source) for source, target in forward]
        low = lax.ppermute(
            lax.slice_in_dim(block, block.shape[dim] - width, None, axis=dim), axis, forward
        )
        high = lax.ppermute(lax.slice_in_dim(block, 0, width, axis=dim), axis, backward)
        block = jnp.concatenate([low, block, high], axis=dim)
    return block


def local(
    queries,
    key_rows,
    values,
    sink_logit,
    out_weight,
    out_gain,
    routed_tokens,
    expert_ids,
    route_weight,
    routed_gain,
    expert_gate,
    expert_up,
    expert_down,
):
    row_count = queries.shape[0]
    heads_here = queries.shape[1] // HEAD_DIM
    kv_here = key_rows.shape[1] // HEAD_DIM
    group_size = heads_here // kv_here
    width = out_weight.shape[1]
    paired = jnp.concatenate((key_rows, values), axis=1)
    extended = padded(paired, (("ep", 0),), WINDOW)
    offset = lax.axis_index("ep") * row_count
    seq_total = row_count * lax.axis_size("ep")
    grouped = queries.reshape(row_count, kv_here, group_size, HEAD_DIM)
    sinks = sink_logit.reshape(kv_here, group_size)[:, :, None, None]
    span_keys = QBLOCK + 2 * WINDOW

    def attend_block(block_index):
        start_row = block_index * QBLOCK
        query_block = lax.dynamic_slice_in_dim(grouped, start_row, QBLOCK, 0)
        band = lax.dynamic_slice_in_dim(extended, start_row, span_keys, 0)
        key_block = band[:, : kv_here * HEAD_DIM].reshape(span_keys, kv_here, HEAD_DIM)
        value_block = band[:, kv_here * HEAD_DIM :].reshape(span_keys, kv_here, HEAD_DIM)
        scores = jnp.einsum(
            "qhgd,khd->hgqk", query_block, key_block, preferred_element_type=jnp.float32
        ) * HEAD_DIM ** (-0.5)
        query_pos = offset + start_row + jnp.arange(QBLOCK, dtype=jnp.int32)
        key_pos = offset + start_row - WINDOW + jnp.arange(span_keys, dtype=jnp.int32)
        valid = (
            (jnp.abs(key_pos[None, :] - query_pos[:, None]) <= WINDOW)
            & (key_pos[None, :] >= 0)
            & (key_pos[None, :] < seq_total)
        )
        masked = jnp.where(valid, scores, -1e30)
        largest = jnp.maximum(jnp.max(masked, axis=-1, keepdims=True), sinks)
        raised = jnp.where(valid, jnp.exp(masked - largest), 0.0)
        denominator = jnp.sum(raised, axis=-1, keepdims=True) + jnp.exp(sinks - largest)
        weights = (raised / denominator).astype(jnp.bfloat16)
        attended = jnp.einsum(
            "hgqk,khd->qhgd", weights, value_block, preferred_element_type=jnp.float32
        )
        return attended.astype(jnp.bfloat16).reshape(QBLOCK, heads_here * HEAD_DIM)

    attended = lax.map(attend_block, jnp.arange(row_count // QBLOCK, dtype=jnp.int32))
    attended = attended.reshape(row_count, heads_here * HEAD_DIM)
    mixed = lax.psum_scatter(
        jnp.dot(attended, out_weight, preferred_element_type=jnp.float32),
        "tp",
        scatter_dimension=0,
        tiled=True,
    )
    mixer_out = (
        mixed * lax.rsqrt(jnp.mean(mixed * mixed, axis=-1, keepdims=True) + epsilon) * out_gain
    ).astype(jnp.bfloat16)
    token_total = routed_tokens.shape[0]
    inputs = routed_tokens.astype(jnp.float32)
    normed = (
        inputs
        * lax.rsqrt(jnp.mean(inputs * inputs, axis=-1, keepdims=True) + epsilon)
        * routed_gain
    ).astype(jnp.bfloat16)
    flat_ids = expert_ids.reshape(-1)
    onehot = (flat_ids[:, None] == jnp.arange(EXPERTS, dtype=jnp.int32)[None, :]).astype(jnp.int32)
    earlier = jnp.cumsum(onehot, axis=0) - onehot
    slot_index = jnp.sum(earlier * onehot, axis=1)
    flat_dest = slot_index * EXPERTS + flat_ids
    source_rows = jnp.arange(token_total * TOP, dtype=jnp.int32) // TOP
    slot_token = jnp.full((CAP * EXPERTS,), token_total, jnp.int32).at[flat_dest].set(source_rows)
    outgoing = jnp.take(normed, slot_token, axis=0, mode="fill", fill_value=0).reshape(
        1, CAP, EXPERTS, width
    )
    arrived = lax.all_to_all(outgoing, "ep", split_axis=2, concat_axis=0, tiled=True)
    source_count, slot_count, local_experts, feature_count = arrived.shape
    rows_in = arrived.reshape(source_count * slot_count, local_experts, feature_count)
    gate_piece = lax.all_gather(expert_gate, "tp", axis=2, tiled=True)
    up_piece = lax.all_gather(expert_up, "tp", axis=2, tiled=True)
    down_piece = lax.all_gather(expert_down, "tp", axis=2, tiled=True)
    gate = jnp.einsum("red,edf->ref", rows_in, gate_piece, preferred_element_type=jnp.float32)
    upward = jnp.einsum("red,edf->ref", rows_in, up_piece, preferred_element_type=jnp.float32)
    hidden = (jax.nn.silu(gate) * upward).astype(jnp.bfloat16)
    summed = jnp.einsum("ref,edf->red", hidden, down_piece, preferred_element_type=jnp.float32)
    produced = summed.astype(jnp.bfloat16).reshape(
        source_count, slot_count, local_experts, feature_count
    )
    returned = lax.all_to_all(produced, "ep", split_axis=0, concat_axis=2, tiled=True)
    returned = returned.reshape(CAP * EXPERTS, width)
    picked_rows = jnp.take(returned, flat_dest, axis=0).reshape(token_total, TOP, width)
    experts_out = jnp.sum(
        picked_rows.astype(jnp.float32) * route_weight[:, :, None], axis=1
    ).astype(jnp.bfloat16)
    return (mixer_out, experts_out)


def solution(mesh):
    placed = (
        P("ep", "tp"),
        P("ep", "tp"),
        P("ep", "tp"),
        P("tp"),
        P("tp", None),
        P(),
        P(("ep", "tp"), None),
        P(("ep", "tp"), None),
        P(("ep", "tp"), None),
        P(),
        P("ep", None, "tp"),
        P("ep", None, "tp"),
        P("ep", None, "tp"),
    )
    return jax.shard_map(
        local,
        mesh=mesh,
        in_specs=placed,
        out_specs=(P(("ep", "tp"), None), P(("ep", "tp"), None)),
        check_vma=False,
    )
```

profile of v0, /device:TPU:0, one launch (start us, length us, event | category | flops | bytes accessed | tf_op | source)
XLA Modules:
  0.0 414.6 jit_solution(16288588751576607968)
XLA Ops:
  7.2 0.0 all-gather.4.cloned.1.call-start
  7.2 0.7 all-gather.4.cloned.1.call-update
  7.9 0.0 all-gather.6.cloned.1.call-start
  8.0 0.7 all-gather.6.cloned.1.call-update
  8.7 0.8 copy.50
  9.5 0.2 eq.29
  9.7 0.2 eq.25
  9.8 0.2 reshape.288
  10.0 9.0 %reduce-window.6 = s32[32,8,128]{2,1,0:T(8,128)S(1)} reduce-window(s32[32,8,128]{2,1,0:T(8,128)S(1)} %fusion.35, s32[]{:T(128)} %constant.129.clone.1), window={size=1x1x128 pad=0_0x0_0x127_0}, to_apply=%region_6.7 | reduce-window | flops 4161536 | bytes 262148 | tf_op jit(solution)/shard_map/reduce-window
  19.1 0.1 slice.34
  19.2 0.1 copy.52
  19.3 0.1 copy.53
  19.4 0.1 broadcast_add_fusion
  19.6 0.6 copy-done.6
  20.2 4.3 %scatter_custom_fusion = s32[2048]{0:T(1024)S(1)} fusion(s32[1024]{0:T(1024)S(1)} %bitcast.166, s32[1024]{0:T(1024)S(1)} %add_select_fusion, s32[]{:T(128)} %constant.140.clone.1), kind=kCustom, calls=%fused_computation.77 | custom fusion | bytes 8196 | tf_op jit(solution)/shard_map/scatter | solution.py:108
  24.5 0.1 broadcast_in_dim.74
  24.6 0.1 copy.57
  24.7 2.1 fusion.22
  26.9 2.2 fusion.24
  29.0 11.0 %gather_fusion = bf16[2048,2048]{1,0:T(8,128)(2,1)} fusion(bf16[512,2048]{1,0:T(8,128)(2,1)S(1)} %fusion.24, s32[2048]{0:T(1024)S(1)} %fusion.36), kind=kCustom, calls=%fused_computation | custom fusion | bytes 16785408 | tf_op jit(solution)/shard_map/jit(_take)/gather | solution.py:109
  40.0 16.8 %copy_select_fusion = bf16[1,64,32,2048]{3,1,0,2:T(8,128)(2,1)} fusion(bf16[1,64,32,2048]{3,2,1,0:T(8,128)(2,1)} %bitcast.155, pred[64,32]{0,1:T(8,128)(4,1)S(1)} %copy.57), kind=kLoop, calls=%fused_computation.37 | loop fusion | flops 4194304 | bytes 16779264 | tf_op jit(solution)/shard_map/jit(_take)/select_n | solution.py:109
  56.8 8.7 %all-to-all-start = ((bf16[1,64,32,2048]{3,1,0,2:T(8,128)(2,1)}), bf16[1,64,32,2048]{3,1,0,2:T(8,128)(2,1)}, u32[]{:S(2)}, u32[]{:S(2)}) async-start(bf16[1,64,32,2048]{3,1,0,2:T(8,128)(2,1)} %copy_select_fusion), calls=%async_computation.1 | async-start | bytes 16777216 | tf_op jit(solution)/shard_map/all_to_all | solution.py:112
  65.5 0.0 all-gather.8.cloned.1.call-start
  65.6 2.1 collective-permute-start
  67.7 1.3 collective-permute-start.1
  69.0 0.2 reduce-scatter.2.cloned.1.call-start
  69.3 1.3 copy.48
  70.6 1.4 collective-permute-done.1
  72.0 25.4 %while.12 = (s32[]{:T(128)}, bf16[2,512,256]{2,1,0:T(8,128)(2,1)S(1)}, s32[2]{0:T(128)S(1)}, bf16[1280,128]{0,1:T(8,128)(2,1)S(1)}, s32[]{:T(128)}, /*index=5*/b...) while((s32[]{:T(128)}, ...), condition=%wide.region_3.4_spmd, body=%wide.region_0.3_spmd.sunk | while | flops 426778112 | bytes 47478104 | solution.py:84
  72.0 0.6 dynamic_slice.28
  73.2 0.8 fusion.57
  74.0 1.2 fusion.58
  75.2 0.1 broadcast_maximum_fusion.2
  75.3 2.6 copy-done.2
  77.8 1.6 fusion.59
  79.4 0.1 exponential_add_fusion.2
  79.5 5.0 %fusion.60 = bf16[64,4,512]{2,0,1:T(8,128)(2,1)S(1)} fusion(f32[4,512]{1,0:T(4,128)S(1)} %exponential_add_fusion.2, f32[4,512]{1,0:T(4,128)S(1)} %broadcast_maximum_fusion.2, f32[768,512,4]{1,0,2:T(8,128)} %copy-done.2, pred[512,768]{0,1:T(8,128)(4,1)S(1)} %fusion.57, bf16[1280,128]{0,1:T(8,128)(2,1)S(1)} %get-tuple-element.194, s32[]{:T(128)S(6)} %select_n.125, ...), kind=kOutput, calls=%fused_computation.13.clone.1 | convolution fusion | flops 210894848 | bytes 7061512 | tf_op jit(solution)/shard_map/while/body/eval_jaxpr/hgqk,khd->qhgd/dot_general | solution.py:79
  84.5 0.1 copy.69
  84.7 0.6 dynamic_slice.28
  85.9 0.8 fusion.57
  86.6 1.2 fusion.58
  87.9 0.1 broadcast_maximum_fusion.2
  88.0 2.6 copy-done.2
  90.5 1.6 fusion.59
  92.1 0.1 exponential_add_fusion.2
  92.2 5.0 %fusion.60 = bf16[64,4,512]{2,0,1:T(8,128)(2,1)S(1)} fusion(f32[4,512]{1,0:T(4,128)S(1)} %exponential_add_fusion.2, f32[4,512]{1,0:T(4,128)S(1)} %broadcast_maximum_fusion.2, f32[768,512,4]{1,0,2:T(8,128)} %copy-done.2, pred[512,768]{0,1:T(8,128)(4,1)S(1)} %fusion.57, bf16[1280,128]{0,1:T(8,128)(2,1)S(1)} %get-tuple-element.194, s32[]{:T(128)S(6)} %select_n.125, ...), kind=kOutput, calls=%fused_computation.13.clone.1 | convolution fusion | flops 210894848 | bytes 7061512 | tf_op jit(solution)/shard_map/while/body/eval_jaxpr/hgqk,khd->qhgd/dot_general | solution.py:79
  97.2 0.1 copy.69
  97.4 4.5 %fusion.44 = f32[1024,2048]{1,0:T(8,128)} fusion(bf16[1024,256]{1,0:T(8,128)(2,1)S(1)} %bitcast.159, bf16[256,2048]{1,0:T(8,128)(2,1)S(1)} %copy-done), kind=kOutput, calls=%fused_computation.86 | convolution fusion | flops 1073741824 | bytes 9961472 | tf_op jit(solution)/shard_map/dot_general | solution.py:87
  101.9 0.0 all-gather.4.cloned.1.call-done
  102.0 69.7 %all-to-all-done = bf16[1,64,32,2048]{3,1,0,2:T(8,128)(2,1)} async-done(((bf16[1,64,32,2048]{3,1,0,2:T(8,128)(2,1)}), bf16[1,64,32,2048]{3,1,0,2:T(8,128)(2,1)}, u32[]{:S(2)}, u32[]{:S(2)}) %all-to-all-start) | async-done | bytes 8388640 | tf_op jit(solution)/shard_map/all_to_all | solution.py:112
  171.7 14.4 %fusion.29 = f32[2048,1024]{1,0:T(8,128)} fusion(bf16[2048,2048]{1,0:T(8,128)(2,1)} %bitcast.21, bf16[1,2048,1024]{2,1,0:T(8,128)(2,1)} %all-gather.4.cloned.1.call-done), kind=kOutput, calls=%fused_computation.49 | convolution fusion | flops 8589934592 | bytes 20971520 | tf_op jit(solution)/shard_map/red,edf->ref/dot_general | solution.py:118
  186.1 26.2 %convolution_convert_fusion = bf16[2048,2048]{1,0:T(8,128)(2,1)} fusion(bf16[1,2048,1024]{2,1,0:T(8,128)(2,1)} %all-gather.8.cloned.1.call-done, f32[2048,1024]{1,0:T(8,128)} %fusion.29, bf16[2048,2048]{1,0:T(8,128)(2,1)} %bitcast.21, bf16[1,2048,1024]{2,1,0:T(8,128)(2,1)} %all-gather.6.cloned.1.call-done), kind=kOutput, calls=%fused_computation.40 | convolution fusion | flops 17196646400 | bytes 33554432 | tf_op jit(solution)/shard_map/ref,edf->red/dot_general | solution.py:121
  212.3 33.3 %all-to-all-start.1 = ((bf16[32,64,1,2048]{3,1,2,0:T(8,128)(2,1)}), bf16[32,64,1,2048]{3,1,2,0:T(8,128)(2,1)}, u32[]{:S(2)}, u32[]{:S(2)}) async-start(bf16[32,64,1,2048]{3,1,2,0:T(8,128)(2,1)} %bitcast.156), calls=%async_computation.2 | async-start | bytes 16777216 | tf_op jit(solution)/shard_map/all_to_all | solution.py:125
  245.6 0.2 mul.111
  245.8 0.1 copy.54
  246.0 0.2 copy.55
  246.2 0.1 copy.61
  246.3 104.9 %all-to-all-done.1 = bf16[32,64,1,2048]{3,1,2,0:T(8,128)(2,1)} async-done(((bf16[32,64,1,2048]{3,1,2,0:T(8,128)(2,1)}), bf16[32,64,1,2048]{3,1,2,0:T(8,128)(2,1)}, u32[]{:S(2)}, u32[]{:S(2)}) %all-to-all-start.1) | async-done | bytes 8388640 | tf_op jit(solution)/shard_map/all_to_all | solution.py:125
  351.2 11.2 %copy.60 = bf16[1,64,32,1,2048]{4,2,1,3,0:T(8,128)(2,1)} copy(bf16[1,64,32,1,2048]{4,1,2,3,0:T(8,128)(2,1)} %bitcast.42) | data formatting | bytes 16777216 | tf_op jit(solution)/shard_map/all_to_all | solution.py:125
  362.4 13.3 %gather_fusion.1 = bf16[1024,2048]{1,0:T(8,128)(2,1)} fusion(bf16[2048,2048]{1,0:T(8,128)(2,1)} %bitcast.154, s32[1024]{0:T(1024)S(1)} %broadcast_clamp_fusion), kind=kCustom, calls=%fused_computation.1 | custom fusion | bytes 8392704 | tf_op jit(solution)/shard_map/jit(_take)/gather | solution.py:127
  375.7 7.7 %gather.15 = bf16[512,2,2048]{2,1,0:T(2,128)(2,1)} reshape(bf16[1024,2048]{1,0:T(8,128)(2,1)} %gather_fusion.1) | data formatting | bytes 8388608 | tf_op jit(solution)/shard_map/jit(_take)/gather | solution.py:127
  383.4 20.0 %multiply_reduce_fusion = bf16[512,2048]{1,0:T(8,128)(2,1)} fusion(bf16[512,2,2048]{2,1,0:T(2,128)(2,1)} %gather.15, pred[512,2]{1,0:T(8,128)(4,1)S(1)} %copy.55, f32[512,2]{1,0:T(8,128)S(1)} %copy.61), kind=kLoop, calls=%fused_computation.38 | loop fusion | flops 7340032 | bytes 6296576 | tf_op jit(solution)/shard_map/reduce_sum | solution.py:128
  403.5 1.8 multiply_reduce_fusion.1
  405.3 2.8 multiply_convert_fusion
  (60 shorter events, 0.4 us)
Async XLA Ops:
  7.2 90.2 %copy-start = (bf16[256,2048]{1,0:T(8,128)(2,1)S(1)}, bf16[256,2048]{1,0:T(8,128)(2,1)}, u32[]{:S(2)}) copy-start(bf16[256,2048]{1,0:T(8,128)(2,1)} %param.19) | copy-start | bytes 3145732
  7.2 19.7 %copy-start.11 = (f32[2048]{0:T(1024)S(1)}, f32[2048]{0:T(1024)}, u32[]{:S(2)}) copy-start(f32[2048]{0:T(1024)} %param.24) | copy-start | bytes 24580
  7.2 94.8 %all-gather.4.cloned.1.call-start = ((), (), s32[]{:S(2)}) async-start(), calls=%async_computation.4 | async-start | bytes 5242880 | tf_op jit(solution)/shard_map/all_gather | solution.py:115
  7.9 178.2 %all-gather.6.cloned.1.call-start = ((), (), s32[]{:S(2)}) async-start(), calls=%async_computation.5 | async-start | bytes 5242880 | tf_op jit(solution)/shard_map/all_gather | solution.py:116
  19.6 0.6 copy-start.6
  20.2 4.3 %copy-start.9 = (s32[1024,1]{0,1:T(1,128)}, s32[1024,1]{0,1:T(1,128)S(1)}, u32[]{:S(2)}) copy-start(s32[1024,1]{0,1:T(1,128)S(1)} %compare_select_fusion) | copy-start | bytes 12292
  56.8 8.8 %copy-start.3 = (bf16[1024,64]{0,1:T(8,128)(2,1)S(1)}, bf16[1024,64]{0,1:T(8,128)(2,1)}, u32[]{:S(2)}) copy-start(bf16[1024,64]{0,1:T(8,128)(2,1)} %param.16) | copy-start | bytes 393220
  56.8 8.8 %copy-start.4 = (bf16[1024,64]{0,1:T(8,128)(2,1)S(1)}, bf16[1024,64]{0,1:T(8,128)(2,1)}, u32[]{:S(2)}) copy-start(bf16[1024,64]{0,1:T(8,128)(2,1)} %param.17) | copy-start | bytes 393220
  56.8 15.2 %copy-start.5 = (f32[4]{0:T(128)S(1)}, f32[4]{0:T(128)}, u32[]{:S(2)}) copy-start(f32[4]{0:T(128)} %param.18) | copy-start | bytes 52
  56.8 114.9 %all-to-all-start = ((bf16[1,64,32,2048]{3,1,0,2:T(8,128)(2,1)}), bf16[1,64,32,2048]{3,1,0,2:T(8,128)(2,1)}, u32[]{:S(2)}, u32[]{:S(2)}) async-start(bf16[1,64,32,2048]{3,1,0,2:T(8,128)(2,1)} %copy_select_fusion), calls=%async_computation.1 | async-start | bytes 16777216 | tf_op jit(solution)/shard_map/all_to_all | solution.py:112
  65.5 120.6 %all-gather.8.cloned.1.call-start = ((), (), s32[]{:S(2)}) async-start(), calls=%async_computation.6 | async-start | bytes 5242880 | tf_op jit(solution)/shard_map/all_gather | solution.py:117
  65.6 4.9 %collective-permute-start = (bf16[128,128]{0,1:T(8,128)(2,1)S(1)}, bf16[128,128]{0,1:T(8,128)(2,1)S(1)}, u32[]{:S(2)}, u32[]{:S(2)}) collective-permute-start(bf16[128,128]{0,1:T(8,128)(2,1)S(1)} %get-tuple-element.110), channel_id=1, source_target_pairs={{0,4},{4,8},{8,12},{12,16},{16,20},{20,24},{24,28},{28,32},{32,36}... | collective-permute-start | bytes 98312 | tf_op jit(solution)/shard_map/ppermute | solution.py:22
  67.7 4.2 %collective-permute-start.1 = (bf16[128,128]{0,1:T(8,128)(2,1)S(1)}, bf16[128,128]{0,1:T(8,128)(2,1)S(1)}, u32[]{:S(2)}, u32[]{:S(2)}) collective-permute-start(bf16[128,128]{0,1:T(8,128)(2,1)S(1)} %get-tuple-element.111), channel_id=1, source_target_pairs={{4,0},{8,4},{12,8},{16,12},{20,16},{24,20},{28,24},{32,28},{36,32}... | collective-permute-start | bytes 98312 | tf_op jit(solution)/shard_map/ppermute | solution.py:25
  69.0 334.4 %reduce-scatter.2.cloned.1.call-start = ((), (), s32[]{:S(2)}) async-start(), calls=%async_computation.3 | async-start | bytes 10485760 | tf_op jit(solution)/shard_map/reduce_scatter | solution.py:86
  75.2 2.7 copy-start.2
  87.9 2.7 copy-start.2
  212.3 33.3 %copy-start.7 = (s32[1024]{0:T(1024)S(1)}, s32[1024]{0:T(1024)}, u32[]{:S(2)}) copy-start(s32[1024]{0:T(1024)} %copy-done.6) | copy-start | bytes 12292
  212.3 33.6 %copy-start.8 = (s32[512,2]{0,1:T(2,128)S(1)}, s32[512,2]{0,1:T(2,128)}, u32[]{:S(2)}) copy-start(s32[512,2]{0,1:T(2,128)} %param.22) | copy-start | bytes 12292
  212.3 33.8 %copy-start.13 = (f32[512,2]{0,1:T(2,128)S(1)}, f32[512,2]{0,1:T(2,128)}, u32[]{:S(2)}) copy-start(f32[512,2]{0,1:T(2,128)} %param.23) | copy-start | bytes 12292
  212.3 34.0 %copy-start.10 = (s32[1024,1]{0,1:T(1,128)S(1)}, s32[1024,1]{0,1:T(1,128)}, u32[]{:S(2)}) copy-start(s32[1024,1]{0,1:T(1,128)} %copy-done.9) | copy-start | bytes 12292
  212.3 138.9 %all-to-all-start.1 = ((bf16[32,64,1,2048]{3,1,2,0:T(8,128)(2,1)}), bf16[32,64,1,2048]{3,1,2,0:T(8,128)(2,1)}, u32[]{:S(2)}, u32[]{:S(2)}) async-start(bf16[32,64,1,2048]{3,1,2,0:T(8,128)(2,1)} %bitcast.156), calls=%async_computation.2 | async-start | bytes 16777216 | tf_op jit(solution)/shard_map/all_to_all | solution.py:125
  375.7 32.4 %copy-start.1 = (bf16[256,2048]{1,0:T(8,128)(2,1)S(1)}, bf16[256,2048]{1,0:T(8,128)(2,1)}, u32[]{:S(2)}) copy-start(bf16[256,2048]{1,0:T(8,128)(2,1)} %param.19) | copy-start | bytes 3145732
  383.4 21.9 %copy-start.12 = (f32[2048]{0:T(1024)S(1)}, f32[2048]{0:T(1024)}, u32[]{:S(2)}) copy-start(f32[2048]{0:T(1024)} %param.20) | copy-start | bytes 24580
Sparse Core Ops, SparseCore 0:
  9.7 53.8 all-gather.3
  65.2 52.2 all-gather.5
  119.2 52.2 all-gather.7
  173.9 105.0 reduce-scatter.1
where the time goes:
time: 416 us; the launch traced here: 415 us
  waiting for transfers between devices  177 us (43%)
  other arithmetic  60 us (14%)
  local copies, waits for them, and re-layouts  58.5 us (14%)
  matrix products  57.6 us (14%)
  starting transfers between devices  45.7 us (11%)
  between operations  14.1 us (3%)
    all_to_all x1, waiting for transfers between devices, local(): lax.all_to_all(produced, 'ep', split_axis=0, concat_axis=2, tiled=True)  105 us
    all_to_all x1, waiting for transfers between devices, local(): lax.all_to_all(outgoing, 'ep', split_axis=2, concat_axis=0, tiled=True)  69.7 us
    all_to_all x1, starting transfers between devices, local(): lax.all_to_all(produced, 'ep', split_axis=0, concat_axis=2, tiled=True)  33.3 us
    dot_general x1, matrix products, local(): jnp.einsum('ref,edf->red', hidden, down_piece, preferred_element_type=jnp...  26.2 us
    gather x2, local copies, waits for them, and re-layouts, local(): jnp.take(returned, flat_dest, axis=0).reshape(token_total, TOP, width)  21 us
    reduce_sum x1, other arithmetic, local(): jnp.sum(picked_rows.astype(jnp.float32) * route_weight[:, :, None], axis=1)  20 us
    select_n x1, other arithmetic, local(): jnp.take(normed, slot_token, axis=0, mode='fill', fill_value=0)  16.8 us
    dot_general x1, matrix products, local(): jnp.einsum('red,edf->ref', rows_in, gate_piece, preferred_element_type=jn...  14.4 us
  transfers between devices with their start and end apart: 8, of which 3 were waited for; matrix products, arithmetic and copies ran while one was open for 40% of the time, Pallas kernels for 0%

commit v1 on v0

v1 whole, which is shorter than its diff:
```python
import jax
import jax.numpy as jnp
from jax import lax
from jax.experimental import pallas as pl
from jax.experimental.pallas import tpu as pltpu
from jax.sharding import PartitionSpec as P

F32, BF16 = jnp.float32, jnp.bfloat16
MESH = pl.DeviceIdType.MESH
D = 2048
WINDOW = 128
SEQ = 32768
EPS = 1e-06
COPIES = 128


def dot(a, b):
    return lax.dot_general(a, b, (((1,), (0,)), ((), ())), preferred_element_type=F32)


def dot_nt(a, b):
    return lax.dot_general(a, b, (((1,), (1,)), ((), ())), preferred_element_type=F32)


def iota(shape, dim):
    return lax.broadcasted_iota(jnp.int32, shape, dim)


def kernel(
    q_in, kv_in, sink, ow_in, og, tok_in, meta, rg, wg_in, wu_in, wd_in,
    mix_out, exp_out,
    W, OW, T, X, H, R, FB, S, OUT, WS, PT, PM, MT, MS, Q, KV, ATT, AR, MX,
    ready, lsem, ssem, rsem,
):
    ep = lax.axis_index("ep")
    tp = lax.axis_index("tp")
    core, y, z = ep % 2, (ep // 2) % 4, ep // 8

    def place(z, y, core):
        return (z * 4 + y) * 2 + core

    xr, xl, xo = (ep, (tp + 1) % 4), (ep, (tp + 3) % 4), (ep, (tp + 2) % 4)
    yr, yl = (place(z, (y + 1) % 4, core), tp), (place(z, (y + 3) % 4, core), tp)
    zr, zl, zo = (
        (place((z + 1) % 4, y, core), tp),
        (place((z + 3) % 4, y, core), tp),
        (place((z + 2) % 4, y, core), tp),
    )
    sib = (place(z, y, 1 - core), tp)
    after, before = ((ep + 1) % 32, tp), ((ep + 31) % 32, tp)

    numbers = {}
    unsent = {}

    def send(name, src, dst, dev):
        n = numbers.setdefault(name, len(numbers))
        copy = pltpu.make_async_remote_copy(
            src_ref=src, dst_ref=dst, send_sem=ssem.at[n], recv_sem=rsem.at[n],
            device_id=dev, device_id_type=MESH,
        )
        copy.start()
        unsent[name] = copy
        copies[name] = copy

    copies = {}

    def got(name):
        copies[name].wait_recv()

    def sent(prefix):
        for name in [n for n in unsent if n.startswith(prefix)]:
            unsent.pop(name).wait_send()

    here = [
        pltpu.make_async_copy(src, dst, lsem.at[i])
        for i, (src, dst) in enumerate([
            (wg_in, W.at[0, 0]),
            (wu_in, W.at[1, 0]),
            (wd_in, W.at[2, 0]),
            (tok_in, X.at[3]),
            (kv_in, KV.at[WINDOW : WINDOW + 1024]),
            (q_in, Q),
            (ow_in, OW.at[0]),
        ])
    ]
    for copy in here:
        copy.start()
    barrier = pltpu.get_barrier_semaphore()
    near = (xr, xl, xo, yr, yl, zr, zl, zo, sib, after, before)
    for dev in near:
        pl.semaphore_signal(barrier, inc=1, device_id=dev, device_id_type=MESH)
    pl.semaphore_wait(barrier, len(near))

    for m in range(3):
        here[m].wait()
        send(f"x{m}r", W.at[m, 0], W.at[m, 1], xr)
        send(f"x{m}l", W.at[m, 0], W.at[m, 2], xl)

    def pass_weight(m):
        got(f"x{m}r")
        send(f"x{m}fr", W.at[m, 1, 0:1024], W.at[m, 3, 0:1024], xr)
        got(f"x{m}l")
        send(f"x{m}fl", W.at[m, 2, 1024:2048], W.at[m, 3, 1024:2048], xl)

    here[4].wait()
    send("halo_n", KV.at[1024 : 1024 + WINDOW], KV.at[0:WINDOW], after)
    send("halo_p", KV.at[WINDOW : 2 * WINDOW], KV.at[1024 + WINDOW :], before)

    id0, id1 = meta[0:1, :], meta[1:2, :]
    w0, w1 = meta[2:3, :], meta[3:4, :]
    ie = iota((32, 512), 0).astype(F32)
    one0 = jnp.where(ie == id0, 1.0, 0.0)
    one1 = jnp.where(ie == id1, 1.0, 0.0)
    upper = jnp.where(iota((512, 512), 0) < iota((512, 512), 1), 1.0, 0.0).astype(BF16)
    ahead = dot((one0 + one1).astype(BF16), upper)
    slot0 = jnp.sum(ahead * one0, axis=0, keepdims=True)
    slot1 = jnp.sum(ahead * one1, axis=0, keepdims=True) + jnp.where(id0 == id1, 1.0, 0.0)
    gid = jnp.floor(id0 * 0.125)
    oneg = jnp.where(iota((8, 512), 0).astype(F32) == gid, 1.0, 0.0)
    rank = jnp.sum(dot(oneg.astype(BF16), upper) * oneg, axis=0, keepdims=True)
    dest = gid * 128.0 + rank

    def split(w):
        high = w.astype(BF16).astype(F32)
        mid = (w - high).astype(BF16).astype(F32)
        return high, mid, w - high - mid

    rows16 = iota((16, 512), 0)
    m16 = jnp.zeros((16, 512), F32)
    for i, row in enumerate((id0, slot0, id1, slot1, *split(w0), *split(w1))):
        m16 = jnp.where(rows16 == i, row, m16)
    m16 = m16.astype(BF16)
    for kp in range(4):
        base = ((z + kp) % 4) * 128
        pm = jnp.where((iota((128, 512), 0) + base).astype(F32) == dest, 1.0, 0.0)
        PM[kp] = pm.astype(BF16)
        moved = dot_nt(m16, pm.astype(BF16))
        if kp == 0:
            MT[0, 0, 0] = moved
        else:
            MS[kp - 1] = moved
    for kp, dev in ((1, zr), (3, zl), (2, zo)):
        send(f"mz{kp}", MS.at[kp - 1], MT.at[0, 0, (4 - kp) % 4], dev)

    here[3].wait()

    @pl.loop(0, 16)
    def _(i):
        r = pl.ds(pl.multiple_of(i * 32, 32), 32)
        v = X[3, r, :].astype(F32)
        scale = lax.rsqrt(jnp.mean(v * v, axis=-1, keepdims=True) + EPS)
        X[2, r, :] = (v * scale * rg[...]).astype(BF16)

    for kp in (0, 1, 3, 2):
        @pl.loop(0, 4)
        def _(n):
            c = pl.ds(pl.multiple_of(n * 512, 512), 512)
            tile = dot(PM[kp], X[2, :, c]).astype(BF16)
            if kp == 0:
                T[0, 0, 0:128, c] = tile
            else:
                S[kp - 1, :, c] = tile

        if kp:
            dev = {1: zr, 2: zo, 3: zl}[kp]
            send(f"z{kp}", S.at[kp - 1], T.at[(4 - kp) % 4, 0, 0:128], dev)
        else:
            send("y0r", T.at[0, 0, 0:128], T.at[0, 3, 0:128], yr)
            send("y0l", T.at[0, 0, 0:128], T.at[0, 1, 0:128], yl)
            send("d00", T.at[0, 0, 0:128], T.at[0, 0, 128:256], sib)

    def gather_start(k):
        got(f"z{(4 - k) % 4}")
        send(f"y{k}r", T.at[k, 0, 0:128], T.at[k, 3, 0:128], yr)
        send(f"y{k}l", T.at[k, 0, 0:128], T.at[k, 1, 0:128], yl)
        send(f"d{k}0", T.at[k, 0, 0:128], T.at[k, 0, 128:256], sib)

    def gather_pass(k):
        got(f"y{k}r")
        send(f"y{k}fr", T.at[k, 3, 0:64], T.at[k, 2, 0:64], yr)
        send(f"d{k}3", T.at[k, 3, 0:128], T.at[k, 3, 128:256], sib)
        got(f"y{k}l")
        send(f"y{k}fl", T.at[k, 1, 64:128], T.at[k, 2, 64:128], yl)
        send(f"d{k}1", T.at[k, 1, 0:128], T.at[k, 1, 128:256], sib)

    def gather_end(k):
        got(f"y{k}fr")
        got(f"y{k}fl")
        send(f"d{k}2", T.at[k, 2, 0:128], T.at[k, 2, 128:256], sib)

    for kp in (1, 3, 2):
        got(f"mz{kp}")
    send("myr", MT.at[0, 0], MT.at[0, 3], yr)
    send("myl", MT.at[0, 0], MT.at[0, 1], yl)

    here[5].wait()
    got("halo_n")
    got("halo_p")
    lane = iota((128, 128), 1)
    r_pos = iota((128, 384), 0)
    c_pos = iota((128, 384), 1)
    gap = c_pos - r_pos

    @pl.loop(0, 8)
    def _(b):
        r0 = pl.multiple_of(b * 128, 128)
        kk = KV[pl.ds(r0, 384), 0:128]
        vv = KV[pl.ds(r0, 384), 128:256]
        key = c_pos + (ep * 1024 + b * 128 - WINDOW)
        valid = (gap >= 0) & (gap <= 2 * WINDOW) & (key >= 0) & (key < SEQ)
        found = []
        for h in range(4):
            qh = Q[pl.ds(r0, 128), (h // 2) * 128 : (h // 2) * 128 + 128]
            qh = jnp.where((lane < 64) if h % 2 == 0 else (lane >= 64), qh, 0.0).astype(BF16)
            s = dot_nt(qh, kk) * 0.125
            s = jnp.where(valid, s, -1e30)
            largest = jnp.maximum(jnp.max(s, axis=-1, keepdims=True), sink[h])
            e = jnp.where(valid, jnp.exp(s - largest), 0.0)
            total = jnp.sum(e, axis=-1, keepdims=True) + jnp.exp(sink[h] - largest)
            found.append(dot((e / total).astype(BF16), vv))
        ATT[pl.ds(r0, 128), 0:128] = jnp.where(lane < 64, found[0], found[1]).astype(BF16)
        ATT[pl.ds(r0, 128), 128:256] = jnp.where(lane < 64, found[2], found[3]).astype(BF16)

    got("myr")
    send("myf", MT.at[0, 3], MT.at[0, 2], yr)
    got("myl")

    me = ep.astype(F32)

    def pack(k):
        @pl.loop(0, 4)
        def _(j):
            m0, m1 = MT[0, j, k], MT[1, j, k]
            both = jnp.concatenate([m0, m1], axis=1)
            shift = jnp.where(iota((1, 256), 1) >= 128, 64.0, 0.0)
            sl0 = jnp.where(both[0:1] == me, both[1:2] + shift, -1.0)
            sl1 = jnp.where(both[2:3] == me, both[3:4] + shift, -1.0)
            wt0 = both[4:5] + both[5:6] + both[6:7]
            wt1 = both[7:8] + both[8:9] + both[9:10]
            rows = iota((128, 256), 0).astype(F32)
            is0, is1 = rows == sl0, rows == sl1
            pick = jnp.where(is0 | is1, 1.0, 0.0)
            weight = jnp.sum(jnp.where(is0, wt0, 0.0) + jnp.where(is1, wt1, 0.0), axis=1, keepdims=True)
            r = pl.ds(pl.multiple_of(j * 128, 128), 128)
            WS[k, r, :] = jnp.broadcast_to(weight, (128, 128))
            PT[k, j] = jnp.transpose(pick).astype(BF16)
            pick = pick.astype(BF16)
            for n in range(4):
                X[k, r, n * 512 : n * 512 + 512] = dot(
                    pick, T[k, j, :, n * 512 : n * 512 + 512]
                ).astype(BF16)

    def gate_up(first, last):
        @pl.loop(first * 4, last * 4)
        def _(i):
            s, k = i // 4, i % 4
            g = dot(X[k], W[0, s])
            u = dot(X[k], W[1, s])
            H[k, s] = (g / (1.0 + jnp.exp(-g)) * u).astype(BF16)

    gather_pass(0)
    gather_start(1)
    gather_start(3)
    pass_weight(0)
    gather_end(0)
    got("myf")
    send("md", MT.at[0], MT.at[1], sib)
    got("md")
    for j in (0, 3, 1, 2):
        got(f"d0{j}")
    pack(0)
    gather_start(2)
    gather_pass(1)
    gather_end(1)
    pass_weight(1)
    for j in (0, 3, 1, 2):
        got(f"d1{j}")
    pack(1)
    gather_pass(3)
    gather_end(3)
    for j in (0, 3, 1, 2):
        got(f"d3{j}")
    pack(3)
    gather_pass(2)
    pass_weight(2)
    here[6].wait()
    send("owr", OW.at[0], OW.at[1], xr)
    send("owl", OW.at[0], OW.at[2], xl)
    for name, d, slot, dev in (("ar", 1, 1, xr), ("al", 3, 2, xl), ("ao", 2, 3, xo)):
        part = pl.ds(pl.multiple_of(((tp + d) % 4) * 256, 256), 256)
        send(name, ATT.at[part], AR.at[slot], dev)
    gather_end(2)
    for j in (0, 3, 1, 2):
        got(f"d2{j}")
    pack(2)
    sent("y")
    sent("d")
    pl.semaphore_signal(ready, inc=1, device_id=sib, device_id_type=MESH)
    gate_up(0, 3)
    for m in (0, 1):
        got(f"x{m}fr")
        got(f"x{m}fl")
    gate_up(3, 4)
    got("x2fr")
    got("x2fl")
    pl.semaphore_wait(ready, 1)

    def down(k):
        @pl.loop(0, 8)
        def _(n):
            c = pl.ds(pl.multiple_of(n * 256, 256), 256)
            out = dot_nt(H[k, 0], W[2, 0, c, :])
            for s in range(1, 4):
                out += dot_nt(H[k, s], W[2, s, c, :])
            scale = WS[k]
            scale = jnp.concatenate([scale, scale], axis=1)
            scaled = (out.astype(BF16).astype(F32) * scale).astype(BF16)
            for j in range(4):
                part = dot(PT[k, j], scaled[j * 128 : j * 128 + 128])
                X[k, j * 128 : j * 128 + 128, c] = part[0:128].astype(BF16)
                T[k, j, 128:256, c] = part[128:256].astype(BF16)

        send(f"r{k}", T.at[k, :, 128:256], T.at[k, :, 0:128], sib)

    def plus(count, out, *terms):
        @pl.loop(0, count // 16)
        def _(i):
            r = pl.multiple_of(i * 16, 16)
            total = None
            for ref, lead, base in terms:
                term = ref[(*lead, pl.ds(base + r, 16), slice(None))].astype(F32)
                total = term if total is None else total + term
            ref, lead, base = out
            ref[(*lead, pl.ds(base + r, 16), slice(None))] = total.astype(BF16)

    def early(k):
        got(f"r{k}")
        for j in (2, 1, 3, 0):
            plus(128, (X, (k,), j * 128), (X, (k,), j * 128), (T, (k, j), 0))
            if j == 2:
                send(f"b{k}hr", X.at[k, 256:320], R.at[k, 0], yr)
                send(f"b{k}hl", X.at[k, 320:384], R.at[k, 1], yl)
            if j == 1:
                send(f"b{k}er", X.at[k, 192:256], FB.at[k, 0, 64:128], yr)
            if j == 3:
                send(f"b{k}el", X.at[k, 384:448], FB.at[k, 1, 0:64], yl)

    def late(k):
        got(f"b{k}hr")
        plus(64, (X, (k,), 128), (X, (k,), 128), (R, (k, 0), 0))
        send(f"b{k}fr", X.at[k, 128:192], FB.at[k, 0, 0:64], yr)
        got(f"b{k}hl")
        plus(64, (X, (k,), 448), (X, (k,), 448), (R, (k, 1), 0))
        send(f"b{k}fl", X.at[k, 448:512], FB.at[k, 1, 64:128], yl)

    def finish(k):
        for half in ("er", "el", "fr", "fl"):
            got(f"b{k}{half}")
        out = (OUT, (0,), 0) if k == 0 else (S, (k - 1,), 0)
        plus(128, out, (X, (k,), 0), (FB, (k, 0), 0), (FB, (k, 1), 0))
        if k:
            send(f"f{k}", S.at[k - 1], OUT.at[(4 - k) % 4], {1: zr, 2: zo, 3: zl}[k])

    sent("z")
    down(2)
    early(2)
    down(1)
    late(2)
    early(1)
    down(3)
    finish(2)
    late(1)
    early(3)
    down(0)
    got("owr")
    send("owfr", OW.at[1, 0:128], OW.at[3, 0:128], xr)
    got("owl")
    send("owfl", OW.at[2, 128:256], OW.at[3, 128:256], xl)
    finish(1)
    late(3)
    early(0)
    late(0)

    for name in ("ar", "al", "ao", "owfr", "owfl"):
        got(name)
    own = pl.multiple_of(tp * 256, 256)
    AR[0] = ATT[pl.ds(own, 256), :]

    @pl.loop(0, 4)
    def _(i):
        r = pl.ds(pl.multiple_of(i * 64, 64), 64)
        mixed = dot(AR[0, r, :], OW[0])
        for s in range(1, 4):
            mixed += dot(AR[s, r, :], OW[s])
        scale = lax.rsqrt(jnp.mean(mixed * mixed, axis=-1, keepdims=True) + EPS)
        MX[r, :] = (mixed * scale * og[...]).astype(BF16)

    back = pltpu.make_async_copy(MX, mix_out, lsem.at[7])
    back.start()
    finish(3)
    for kp in range(4):
        PT[kp // 2, 2 * (kp % 2)] = jnp.transpose(PM[kp, :, 0:256].astype(F32)).astype(BF16)
        PT[kp // 2, 2 * (kp % 2) + 1] = jnp.transpose(PM[kp, :, 256:512].astype(F32)).astype(BF16)
    finish(0)
    for k in (2, 1, 3):
        got(f"f{k}")
    sent("b1")

    @pl.loop(0, 4)
    def _(n):
        c = pl.ds(pl.multiple_of(n * 512, 512), 512)
        for half in range(2):
            total = None
            for kp in range(4):
                part = dot(PT[kp // 2, 2 * (kp % 2) + half], OUT[kp, :, c])
                total = part if total is None else total + part
            X[1, half * 256 : half * 256 + 256, c] = total.astype(BF16)

    home = pltpu.make_async_copy(X.at[1], exp_out, lsem.at[8])
    home.start()
    sent("")
    home.wait()
    back.wait()


def local(
    queries, key_rows, values, sink_logit, out_weight, out_gain, routed_tokens,
    expert_ids, route_weight, routed_gain, expert_gate, expert_up, expert_down,
):
    kv = jnp.concatenate((key_rows, key_rows, values, values), axis=1)
    meta = jnp.concatenate((expert_ids.astype(F32), route_weight), axis=1).T
    anywhere = pl.BlockSpec(memory_space=pl.ANY)
    vmem = pl.BlockSpec(memory_space=pltpu.VMEM)
    smem = pl.BlockSpec(memory_space=pltpu.SMEM)
    scratch = [
        pltpu.VMEM((3, 4, 2048, 256), BF16),
        pltpu.VMEM((4, 256, D), BF16),
        pltpu.VMEM((4, 4, 256, D), BF16),
        pltpu.VMEM((4, 512, D), BF16),
        pltpu.VMEM((4, 4, 512, 256), BF16),
        pltpu.VMEM((4, 2, 64, D), BF16),
        pltpu.VMEM((4, 2, 128, D), BF16),
        pltpu.VMEM((3, 128, D), BF16),
        pltpu.VMEM((4, 128, D), BF16),
        pltpu.VMEM((4, 512, 128), F32),
        pltpu.VMEM((4, 4, 256, 128), BF16),
        pltpu.VMEM((4, 128, 512), BF16),
        pltpu.VMEM((2, 4, 4, 16, 128), F32),
        pltpu.VMEM((3, 16, 128), F32),
        pltpu.VMEM((1024, 256), BF16),
        pltpu.VMEM((1024 + 2 * WINDOW, 256), BF16),
        pltpu.VMEM((1024, 256), BF16),
        pltpu.VMEM((4, 256, 256), BF16),
        pltpu.VMEM((256, D), BF16),
        pltpu.SemaphoreType.REGULAR,
        pltpu.SemaphoreType.DMA((9,)),
        pltpu.SemaphoreType.DMA((COPIES,)),
        pltpu.SemaphoreType.DMA((COPIES,)),
    ]
    return pl.pallas_call(
        kernel,
        out_shape=(
            jax.ShapeDtypeStruct((256, D), BF16),
            jax.ShapeDtypeStruct((512, D), BF16),
        ),
        in_specs=[anywhere, anywhere, smem, anywhere, vmem, anywhere, vmem, vmem, anywhere, anywhere, anywhere],
        out_specs=(anywhere, anywhere),
        scratch_shapes=scratch,
        compiler_params=pltpu.CompilerParams(
            collective_id=0, has_side_effects=True, vmem_limit_bytes=67043328
        ),
        name="block",
    )(
        queries, kv, sink_logit, out_weight, out_gain.reshape(1, D), routed_tokens, meta,
        routed_gain.reshape(1, D), expert_gate.reshape(D, 256), expert_up.reshape(D, 256),
        expert_down.reshape(D, 256),
    )


def solution(mesh):
    placed = (
        P("ep", "tp"), P("ep", "tp"), P("ep", "tp"), P("tp"), P("tp", None), P(),
        P(("ep", "tp"), None), P(("ep", "tp"), None), P(("ep", "tp"), None), P(),
        P("ep", None, "tp"), P("ep", None, "tp"), P("ep", None, "tp"),
    )
    return jax.shard_map(
        local,
        mesh=mesh,
        in_specs=placed,
        out_specs=(P(("ep", "tp"), None), P(("ep", "tp"), None)),
        check_vma=False,
    )
```

time: 416 us -> 218 us (0.52)
  Pallas kernels: 0 us -> 207 us
  waiting for transfers between devices: 177 us -> 0 us
  matrix products: 57.6 us -> 0 us
  other arithmetic: 60 us -> 3.13 us
  local copies, waits for them, and re-layouts: 58.5 us -> 5.92 us
  starting transfers between devices: 45.7 us -> 0 us
  between operations: 14.1 us -> 0.66 us
    pallas_call x0 -> x1, Pallas kernels: none -> 207 us  [local(): pl.pallas_call(kernel, out_shape=(jax.ShapeDtypeStruct((256, D), BF16), j...]
    all_to_all x2 -> x0, waiting for transfers between devices: 175 us -> none  [the longest x1 105 us: local(): lax.all_to_all(produced, 'ep', split_axis=0, concat_axis=2, tiled=True)]
    dot_general x7 -> x0, matrix products: 57.6 us -> none  [the longest x1 26.2 us: local(): jnp.einsum('ref,edf->red', hidden, down_piece, preferred_element_type=jnp...]
    all_to_all x2 -> x0, starting transfers between devices: 42 us -> none  [the longest x1 33.3 us: local(): lax.all_to_all(produced, 'ep', split_axis=0, concat_axis=2, tiled=True)]
    gather x3 -> x0, local copies, waits for them, and re-layouts: 32 us -> none  [the longest x2 21 us: local(): jnp.take(returned, flat_dest, axis=0).reshape(token_total, TOP, width)]
    reduce_sum x6 -> x0, other arithmetic: 27.2 us -> none  [the longest x1 20 us: local(): jnp.sum(picked_rows.astype(jnp.float32) * route_weight[:, :, None], axis=1)]
    select_n x3 -> x0, other arithmetic: 16.8 us -> none  [the longest x1 16.8 us: local(): jnp.take(normed, slot_token, axis=0, mode='fill', fill_value=0)]
    all_to_all x1 -> x0, local copies, waits for them, and re-layouts: 11.2 us -> none  [local(): lax.all_to_all(produced, 'ep', split_axis=0, concat_axis=2, tiled=True)]
  transfers between devices with their start and end apart: 8 -> 0, of which waited for: 3 -> 0; matrix products, arithmetic and copies ran while one was open for 40% -> 0% of each run, Pallas kernels for 0% -> 0%
where the time goes in v1:
time: 218 us; the launch traced here: 217 us
  Pallas kernels  207 us (95%)
  local copies, waits for them, and re-layouts  5.92 us (3%)
  other arithmetic  3.13 us (1%)
    pallas_call x1, Pallas kernels, local(): pl.pallas_call(kernel, out_shape=(jax.ShapeDtypeStruct((256, D), BF16), j...  207 us
    unnamed x6, local copies, waits for them, and re-layouts  5.92 us

profile of v1, /device:TPU:0, one launch (start us, length us, event | category | flops | bytes accessed | tf_op | source)
XLA Modules:
  0.0 216.8 jit_solution(4512802364037788472)
XLA Ops:
  0.6 0.7 convert_element_type.3
  1.3 1.3 maximum_bitcast_fusion.meta
  2.6 1.1 copy.15
  3.7 1.1 copy.17
  4.8 1.1 pad_maximum_fusion.kv_in
  5.9 207.1 %block.1 = (bf16[256,2048]{1,0:T(8,128)(2,1)}, bf16[512,2048]{1,0:T(8,128)(2,1)}) custom-call(bf16[1024,256]{1,0:T(8,128)(2,1)} %q_in.1, bf16[1024,256]{1,0:T(8,128)(2,1)} %pad_maximum_fusion.kv_in, f32[4]{0:T(128)} %sink.1, bf16[256,2048]{1,0:T(8,128)(2,1)} %ow_in.1, f32[1,2048]{1,0:T(1,128)} %bitcast.10, bf16[512,2048]{1,0:T(8,128)(2,1)} %tok_in.1, ...), custom_call_target="tpu_custom_call" | custom-call | tf_op jit(solution)/shard_map/block/pallas_call | solution.py:460
  213.0 0.0 copy-start
  213.0 2.5 %copy.21 = bf16[256,2048]{1,0:T(8,128)(2,1)} copy(bf16[256,2048]{1,0:T(8,128)(2,1)} %get-tuple-element.4) | data formatting | bytes 2097152
  215.5 0.0 copy-done
  215.5 1.3 copy.22
Async XLA Ops:
  213.0 2.5 %copy-start = (bf16[512,2048]{1,0:T(8,128)(2,1)S(1)}, bf16[512,2048]{1,0:T(8,128)(2,1)}, u32[]{:S(2)}) copy-start(bf16[512,2048]{1,0:T(8,128)(2,1)} %get-tuple-element.5) | copy-start | bytes 6291460

commit v2 on v0

v2 whole, which is shorter than its diff:
```python
import jax
import jax.numpy as jnp
from jax import lax
from jax.experimental import pallas as pl
from jax.experimental.pallas import tpu as pltpu
from jax.sharding import PartitionSpec as P

F32, BF16 = jnp.float32, jnp.bfloat16
MESH = pl.DeviceIdType.MESH
D = 2048
WINDOW = 128
SEQ = 32768
EPS = 1e-06
COPIES = 117
SENDS = 56


def dot(a, b):
    return lax.dot_general(a, b, (((1,), (0,)), ((), ())), preferred_element_type=F32)


def dot_nt(a, b):
    return lax.dot_general(a, b, (((1,), (1,)), ((), ())), preferred_element_type=F32)


def iota(shape, dim):
    return lax.broadcasted_iota(jnp.int32, shape, dim)


CHUNKS = ((0, 256), (256, 256), (512, 512), (1024, 512), (1536, 512))


def kernel(
    q_in, k_in, v_in, sink, ow_in, og_in, tok_in, ids, rw, rg_in, wg_in, wu_in, wd_in,
    mix_out, exp_out,
    W, OW, T, X, H, R, FB, S, OUT, WS, PT, PM, PMT, MT, MS, Q, KV, ATT, AR, OG, RG,
    ready, lsem, ssem, rsem,
):
    ep = lax.axis_index("ep")
    tp = lax.axis_index("tp")
    core, y, z = ep % 2, (ep // 2) % 4, ep // 8

    def place(z, y, core):
        return (z * 4 + y) * 2 + core

    xr, xl, xo = (ep, (tp + 1) % 4), (ep, (tp + 3) % 4), (ep, (tp + 2) % 4)
    yr, yl = (place(z, (y + 1) % 4, core), tp), (place(z, (y + 3) % 4, core), tp)
    yo = (place(z, (y + 2) % 4, core), tp)
    zs = {d: (place((z + d) % 4, y, core), tp) for d in (1, 2, 3)}
    sib = (place(z, y, 1 - core), tp)
    after, before = ((ep + 1) % 32, tp), ((ep + 31) % 32, tp)

    numbers, unsent, copies, groups = {}, {}, {}, {}
    free = list(range(SENDS))[::-1]

    def send(name, src, dst, dev, into=None, group=None):
        if group in groups:
            n = groups[group]
        else:
            n = free.pop()
        copy = pltpu.make_async_remote_copy(
            src_ref=src, dst_ref=dst, send_sem=ssem.at[n],
            recv_sem=rsem.at[numbers.setdefault(into or name, len(numbers))],
            device_id=dev, device_id_type=MESH,
        )
        copy.start()
        assert name not in copies
        copies[name] = copy
        if group:
            groups[group] = n
        else:
            unsent[name] = copy, n

    def got(*names):
        for name in names:
            with jax.named_scope("got_" + name):
                copies[name].wait_recv()

    def whole(ref, n, m):
        return pltpu.make_async_remote_copy(
            src_ref=ref, dst_ref=ref, send_sem=ssem.at[n], recv_sem=rsem.at[m],
            device_id=sib, device_id_type=MESH,
        )

    def got_all(into, ref):
        with jax.named_scope("got_" + into):
            whole(ref, 0, numbers[into]).wait_recv()

    def sent(prefix):
        with jax.named_scope("sent_" + prefix):
            for name in [n for n in unsent if n.startswith(prefix)]:
                copy, n = unsent.pop(name)
                copy.wait_send()
                free.append(n)

    def sent_all(group, ref):
        with jax.named_scope("sent_" + group):
            n = groups.pop(group)
            whole(ref, n, 0).wait_send()
            free.append(n)

    def local(i, src, dst):
        copy = pltpu.make_async_copy(src, dst, lsem.at[i])
        copy.start()
        return copy

    here = [
        local(i, src, dst)
        for i, (src, dst) in enumerate([
            (wg_in, W.at[0, 0]),
            (tok_in, X.at[3]),
            (rg_in, RG),
            (wu_in, W.at[1, 0]),
            (q_in, Q),
            (wd_in, W.at[2, 0]),
            (ow_in, OW.at[0]),
            (og_in, OG),
        ])
    ]
    ours = slice(WINDOW, WINDOW + 1024)
    rows_here = [
        local(8 + 2 * i + half, src, KV.at[i, half * 64 : half * 64 + 64, ours])
        for i, src in enumerate((k_in, v_in))
        for half in range(2)
    ]
    near = (xr, xl, xo, yr, yl, yo, zs[1], zs[2], zs[3], sib, after, before)
    barrier = pltpu.get_barrier_semaphore()
    for dev in near:
        pl.semaphore_signal(barrier, inc=1, device_id=dev, device_id_type=MESH)

    def pass_weight(m):
        got(f"x{m}r")
        send(f"x{m}fr", W.at[m, 1, 0:1024], W.at[m, 3, 0:1024], xr, f"x{m}f")
        got(f"x{m}l")
        send(f"x{m}fl", W.at[m, 2, 1024:2048], W.at[m, 3, 1024:2048], xl, f"x{m}f")

    def start_down(c):
        rows = slice(CHUNKS[c][0], sum(CHUNKS[c]))
        send(f"w{c}r", W.at[2, 0, rows], W.at[2, 1, rows], xr)
        send(f"w{c}l", W.at[2, 0, rows], W.at[2, 2, rows], xl)

    def pass_down(c):
        first, width = CHUNKS[c]
        low, high = slice(first, first + width // 2), slice(first + width // 2, first + width)
        got(f"w{c}r")
        send(f"w{c}fr", W.at[2, 1, low], W.at[2, 3, low], xr, f"w{c}f")
        got(f"w{c}l")
        send(f"w{c}fl", W.at[2, 2, high], W.at[2, 3, high], xl, f"w{c}f")

    with jax.named_scope("routing"):
        id0, id1 = ids[0:1, :].astype(F32), ids[1:2, :].astype(F32)
        w0, w1 = rw[0:1, :], rw[1:2, :]
        ie = iota((32, 512), 0).astype(F32)
        one0 = jnp.where(ie == id0, 1.0, 0.0)
        one1 = jnp.where(ie == id1, 1.0, 0.0)
        upper = jnp.where(iota((512, 512), 0) < iota((512, 512), 1), 1.0, 0.0).astype(BF16)
        ahead = dot((one0 + one1).astype(BF16), upper)
        slot0 = jnp.sum(ahead * one0, axis=0, keepdims=True)
        slot1 = jnp.sum(ahead * one1, axis=0, keepdims=True) + jnp.where(id0 == id1, 1.0, 0.0)
        gid = jnp.floor(id0 * 0.125)
        oneg = jnp.where(iota((8, 512), 0).astype(F32) == gid, 1.0, 0.0)
        rank = jnp.sum(dot(oneg.astype(BF16), upper) * oneg, axis=0, keepdims=True)
        dest = gid * 128.0 + rank

        def split(w):
            high = w.astype(BF16).astype(F32)
            mid = (w - high).astype(BF16).astype(F32)
            return high, mid, w - high - mid

        rows16 = iota((16, 512), 0)
        m16 = jnp.zeros((16, 512), F32)
        for i, row in enumerate((id0, slot0, id1, slot1, *split(w0), *split(w1))):
            m16 = jnp.where(rows16 == i, row, m16)
        m16 = m16.astype(BF16)
        for kp in range(4):
            base = ((z + kp) % 4) * 128
            pm = jnp.where((iota((128, 512), 0) + base).astype(F32) == dest, 1.0, 0.0)
            PM[kp] = pm.astype(BF16)
            moved = dot_nt(m16, pm.astype(BF16))
            if kp == 0:
                MT[0, 0, 0] = moved
            else:
                MS[kp - 1] = moved
    with jax.named_scope("barrier"):
        pl.semaphore_wait(barrier, len(near))

    def start_weight(m, copy):
        copy.wait()
        send(f"x{m}r", W.at[m, 0], W.at[m, 1], xr)
        send(f"x{m}l", W.at[m, 0], W.at[m, 2], xl)

    start_weight(0, here[0])
    here[1].wait()
    here[2].wait()
    def shared(k):
        return None if k == 2 else f"d{k}"

    def start_tile(k):
        send(f"y{k}r", T.at[k, 0, 0:128], T.at[k, 3, 0:128], yr)
        send(f"y{k}l", T.at[k, 0, 0:128], T.at[k, 1, 0:128], yl)
        send(f"d{k}0", T.at[k, 0, 0:128], T.at[k, 0, 128:256], sib, shared(k))

    def permute(kp):
        with jax.named_scope(f"permute_{kp}"):
            v = dot(PM[kp], X[3])
            scale = lax.rsqrt(jnp.mean(v * v, axis=-1, keepdims=True) + EPS)
            tile = (v * scale * RG[...]).astype(BF16)
            if kp == 0:
                T[0, 0, 0:128] = tile
            else:
                S[kp - 1] = tile

    def send_tile(kp):
        send(f"z{kp}", S.at[kp - 1], T.at[4 - kp, 0, 0:128], zs[kp])

    permute(0)
    for kp in (1, 3, 2):
        send(f"mz{kp}", MS.at[kp - 1], MT.at[0, 0, 4 - kp], zs[kp], "mz")
    for copy in rows_here:
        copy.wait()
    send("halo_n", KV.at[:, :, 1024 : 1024 + WINDOW], KV.at[:, :, 0:WINDOW], after, "halo")
    send("halo_p", KV.at[:, :, WINDOW : 2 * WINDOW], KV.at[:, :, 1024 + WINDOW :], before, "halo")
    start_tile(0)
    start_weight(1, here[3])
    here[5].wait()
    start_down(0)
    for kp in (1, 3):
        permute(kp)
        send_tile(kp)
    permute(2)

    def gather_start(k):
        got(f"z{4 - k}")
        start_tile(k)

    def gather_pass(k):
        got(f"y{k}r")
        send(f"y{k}fr", T.at[k, 3, 0:64], T.at[k, 2, 0:64], yr, f"y{k}f")
        send(f"d{k}3", T.at[k, 3, 0:128], T.at[k, 3, 128:256], sib, shared(k))
        got(f"y{k}l")
        send(f"y{k}fl", T.at[k, 1, 64:128], T.at[k, 2, 64:128], yl, f"y{k}f")
        send(f"d{k}1", T.at[k, 1, 0:128], T.at[k, 1, 128:256], sib, shared(k))

    def gather_end(k):
        got_all(f"y{k}f", T.at[k, 2, 0:128])
        send(f"d{k}2", T.at[k, 2, 0:128], T.at[k, 2, 128:256], sib, shared(k))

    def attend(first, last):
        lane = iota((128, 128), 1)
        c_pos = iota((128, 384), 1)
        gap = c_pos - iota((128, 384), 0)

        @pl.loop(first, last)
        def _(i):
            b = (i + 1) % 8
            r0 = pl.multiple_of(b * 128, 128)
            kk = KV[0, :, pl.ds(r0, 384)]
            vv = KV[1, :, pl.ds(r0, 384)]
            key = c_pos + (ep * 1024 + b * 128 - WINDOW)
            valid = (gap >= 0) & (gap <= 2 * WINDOW) & (key >= 0) & (key < SEQ)
            found = []
            for h in range(4):
                qh = Q[pl.ds(r0, 128), (h // 2) * 128 : (h // 2) * 128 + 128]
                qh = jnp.where((lane < 64) if h % 2 == 0 else (lane >= 64), qh, 0.0).astype(BF16)
                s = dot(qh, kk) * 0.125
                s = jnp.where(valid, s, -1e30)
                largest = jnp.maximum(jnp.max(s, axis=-1, keepdims=True), sink[h])
                e = jnp.where(valid, jnp.exp(s - largest), 0.0)
                total = jnp.sum(e, axis=-1, keepdims=True) + jnp.exp(sink[h] - largest)
                found.append(dot_nt((e / total).astype(BF16), vv))
            ATT[pl.ds(r0, 128), 0:128] = jnp.where(lane < 64, found[0], found[1]).astype(BF16)
            ATT[pl.ds(r0, 128), 128:256] = jnp.where(lane < 64, found[2], found[3]).astype(BF16)

    me = ep.astype(F32)

    def pack(k, first=0, last=4):
        with jax.named_scope(f"pack_{k}"):
            @pl.loop(first, last)
            def _(j):
                both = jnp.concatenate([MT[0, j, k], MT[1, j, k]], axis=1)
                shift = jnp.where(iota((1, 256), 1) >= 128, 64.0, 0.0)
                sl0 = jnp.where(both[0:1] == me, both[1:2] + shift, -1.0)
                sl1 = jnp.where(both[2:3] == me, both[3:4] + shift, -1.0)
                wt0 = both[4:5] + both[5:6] + both[6:7]
                wt1 = both[7:8] + both[8:9] + both[9:10]
                rows = iota((128, 256), 0).astype(F32)
                is0, is1 = rows == sl0, rows == sl1
                pick = jnp.where(is0 | is1, 1.0, 0.0)
                weight = jnp.sum(jnp.where(is0, wt0, 0.0) + jnp.where(is1, wt1, 0.0), axis=1, keepdims=True)
                r = pl.ds(pl.multiple_of(j * 128, 128), 128)
                WS[k, r, :] = jnp.broadcast_to(weight, (128, 128))
                PT[k, j] = jnp.transpose(pick).astype(BF16)
                pick = pick.astype(BF16)
                for n in range(4):
                    X[k, r, n * 512 : n * 512 + 512] = dot(
                        pick, T[k, j, :, n * 512 : n * 512 + 512]
                    ).astype(BF16)

    def packed(k):
        sent(f"y{k}")
        sent(f"d{k}")
        pl.semaphore_signal(ready.at[k], inc=1, device_id=sib, device_id_type=MESH)

    def pack_all(k):
        got_all(f"d{k}", T.at[k, :, 128:256])
        pack(k)
        packed(k)

    def gate_up(k, first, last, row=0, rows=512):
        with jax.named_scope(f"gate_up_{k}"):
            @pl.loop(first, last)
            def _(s):
                g = dot(X[k, row : row + rows], W[0, s])
                u = dot(X[k, row : row + rows], W[1, s])
                H[k, s, row : row + rows] = (g / (1.0 + jnp.exp(-g)) * u).astype(BF16)

    here[4].wait()
    with jax.named_scope("attend"):
        attend(0, 2)
    got_all("mz", MT.at[0, 0, 1:4])
    send("myr", MT.at[0, 0], MT.at[0, 3], yr, "my")
    send("myl", MT.at[0, 0], MT.at[0, 1], yl, "my")
    send("myo", MT.at[0, 0], MT.at[0, 2], yo, "my")
    with jax.named_scope("attend"):
        attend(2, 6)
    gather_pass(0)
    gather_start(1)
    gather_start(3)
    send_tile(2)
    got_all("halo", KV.at[:, :, 0 : 2 * WINDOW])
    with jax.named_scope("attend"):
        attend(6, 8)
    got_all("my", MT.at[0, 1:4])
    send("md", MT.at[0], MT.at[1], sib)
    with jax.named_scope("turn"):
        for kp in range(4):
            PMT[kp] = jnp.transpose(PM[kp].astype(F32)).astype(BF16)
    gather_end(0)
    got("md")
    pack_all(0)
    gate_up(0, 0, 1)
    pass_weight(0)
    gather_pass(1)
    gather_start(2)
    gather_pass(3)
    pass_weight(1)
    gather_end(1)
    gate_up(0, 1, 3)
    pack_all(1)
    gate_up(1, 0, 3)
    pass_down(0)
    start_down(1)
    gather_pass(2)
    got("d20", "d23", "d21")
    pack(2, 0, 2)
    pack(2, 3, 4)
    gather_end(3)
    gate_up(2, 0, 3, 0, 256)
    pack_all(3)
    for m in range(2):
        got_all(f"x{m}f", W.at[m, 3])
    gate_up(1, 3, 4)

    def down(c, k):
        with jax.named_scope(f"down_{c}{k}"):
            @pl.loop(0, CHUNKS[c][1] // 256)
            def _(n):
                cols = pl.ds(pl.multiple_of(CHUNKS[c][0] + n * 256, 256), 256)
                out = dot_nt(H[k, 0], W[2, 0, cols, :])
                for s in range(1, 4):
                    out += dot_nt(H[k, s], W[2, s, cols, :])
                scale = WS[k]
                scale = jnp.concatenate([scale, scale], axis=1)
                scaled = (out.astype(BF16).astype(F32) * scale).astype(BF16)
                for j in range(4):
                    part = dot(PT[k, j], scaled[j * 128 : j * 128 + 128])
                    X[k, j * 128 : j * 128 + 128, cols] = part[0:128].astype(BF16)
                    T[k, j, 128:256, cols] = part[128:256].astype(BF16)
        if c == 0:
            pl.semaphore_wait(ready.at[k], 1)
        cols = slice(CHUNKS[c][0], sum(CHUNKS[c]))
        send(f"r{c}{k}", T.at[k, :, 128:256, cols], T.at[k, :, 0:128, cols], sib)

    def plus(c, count, out, *terms):
        step = 16384 // CHUNKS[c][1]

        @pl.loop(0, count // step)
        def _(i):
            r = pl.multiple_of(i * step, step)

            def part(ref, lead, base):
                return (ref, (*lead, pl.ds(base + r, step), slice(CHUNKS[c][0], sum(CHUNKS[c]))))

            total = None
            for term in terms:
                ref, at = part(*term)
                value = ref[at].astype(F32)
                total = value if total is None else total + value
            ref, at = part(*out)
            ref[at] = total.astype(BF16)

    def early(c, k):
        cols = slice(CHUNKS[c][0], sum(CHUNKS[c]))
        got(f"r{c}{k}")
        for j in (2, 1, 3, 0):
            plus(c, 128, (X, (k,), j * 128), (X, (k,), j * 128), (T, (k, j), 0))
            if j == 2:
                send(f"b{c}{k}hr", X.at[k, 256:320, cols], R.at[k, 0, :, cols], yr, f"h{c}{k}", f"b{c}{k}")
                send(f"b{c}{k}hl", X.at[k, 320:384, cols], R.at[k, 1, :, cols], yl, f"h{c}{k}", f"b{c}{k}")
            if j == 1:
                send(f"b{c}{k}er", X.at[k, 192:256, cols], FB.at[k, 0, 64:128, cols], yr, f"F{c}{k}", f"b{c}{k}")
            if j == 3:
                send(f"b{c}{k}el", X.at[k, 384:448, cols], FB.at[k, 1, 0:64, cols], yl, f"F{c}{k}", f"b{c}{k}")

    def late(c, k):
        cols = slice(CHUNKS[c][0], sum(CHUNKS[c]))
        got_all(f"h{c}{k}", R.at[k, :, :, cols])
        plus(c, 64, (X, (k,), 128), (X, (k,), 128), (R, (k, 0), 0))
        send(f"b{c}{k}fr", X.at[k, 128:192, cols], FB.at[k, 0, 0:64, cols], yr, f"F{c}{k}", f"b{c}{k}")
        plus(c, 64, (X, (k,), 448), (X, (k,), 448), (R, (k, 1), 0))
        send(f"b{c}{k}fl", X.at[k, 448:512, cols], FB.at[k, 1, 64:128, cols], yl, f"F{c}{k}", f"b{c}{k}")

    def settle():
        unit, ref = done.pop(0)
        sent("r" + unit)
        sent_all("b" + unit, ref)

    def finish(c, k):
        cols = slice(CHUNKS[c][0], sum(CHUNKS[c]))
        got_all(f"F{c}{k}", FB.at[k, :, :, cols])
        out = (OUT, (0,), 0) if k == 0 else (S, (k - 1,), 0)
        plus(c, 128, out, (X, (k,), 0), (FB, (k, 0), 0), (FB, (k, 1), 0))
        if k:
            send(f"f{c}{k}", S.at[k - 1, :, cols], OUT.at[4 - k, :, cols], zs[k], f"f{c}")

        done.append((f"{c}{k}", X.at[k, 128:512, cols]))
        if len(done) > 1:
            settle()

    homes, done = [], []

    def restore(c):
        got_all(f"f{c}", OUT.at[1:4, :, slice(CHUNKS[c][0], sum(CHUNKS[c]))])
        first, width = CHUNKS[c]
        for piece in range(first // 256, (first + width) // 256):
            cols = slice(piece * 256, piece * 256 + 256)
            spot = (0, piece // 4)
            with jax.named_scope(f"restore_{c}"):
                for half in range(2):
                    total = None
                    for kp in range(4):
                        part = dot(PMT[kp, half * 256 : half * 256 + 256], OUT[kp, :, cols])
                        total = part if total is None else total + part
                    base = piece % 4 * 512 + half * 256
                    W[(*spot, slice(base, base + 256), slice(None))] = total.astype(BF16)
            base = piece % 4 * 512
            homes.append(local(20 + piece, W.at[0, piece // 4, base : base + 512], exp_out.at[:, cols]))

    half_rows = pl.ds(pl.multiple_of(core * 128, 128), 128)

    def start_out():
        here[6].wait()
        send("owr", OW.at[0, half_rows], OW.at[1, half_rows], xr)
        send("owl", OW.at[0, half_rows], OW.at[2, half_rows], xl)
        for name, d, slot, dev in (("ar", 1, 1, xr), ("al", 3, 2, xl), ("ao", 2, 3, xo)):
            part = pl.ds(pl.multiple_of(((tp + d) % 4) * 256, 256), 256)
            send(name, ATT.at[part], AR.at[slot], dev, "a")

    def pass_out():
        low = pl.ds(pl.multiple_of(core * 128, 64), 64)
        high = pl.ds(pl.multiple_of(core * 128 + 64, 64), 64)
        got("owr")
        send("owfr", OW.at[1, low], OW.at[3, low], xr, "owf")
        got("owl")
        send("owfl", OW.at[2, high], OW.at[3, high], xl, "owf")

    def share_out():
        got_all("owf", OW.at[3, half_rows])
        send("owd", OW.at[1:4, half_rows], OW.at[1:4, half_rows], sib)

    def project(half):
        if half == 0:
            got_all("a", AR.at[1:4])
            got("owd")
            here[7].wait()
            AR[0] = ATT[pl.ds(pl.multiple_of(tp * 256, 256), 256), :]
        with jax.named_scope("project"):
            r = slice(half * 128, half * 128 + 128)
            mixed = dot(AR[0, r, :], OW[0])
            for s in range(1, 4):
                mixed += dot(AR[s, r, :], OW[s])
            scale = lax.rsqrt(jnp.mean(mixed * mixed, axis=-1, keepdims=True) + EPS)
            mixed = (mixed * scale * OG[...]).astype(BF16)
            for piece in range(8):
                base = piece * 256 + half * 128
                W[1, 0, base : base + 128] = mixed[:, piece * 256 : piece * 256 + 256]
        if half == 1:
            for piece in range(8):
                base = piece * 256
                homes.append(local(12 + piece, W.at[1, 0, base : base + 256], mix_out.at[:, base : base + 256]))

    hooks = {
        0: [lambda: gate_up(0, 3, 4), lambda: gather_end(2)],
        1: [lambda: pass_down(1), lambda: start_down(2), lambda: gate_up(3, 0, 3)],
        2: [lambda: late(*units[0]), lambda: gate_up(3, 3, 4)],
        3: [lambda: start_down(3), lambda: late(*units[1]), lambda: got("d22"), lambda: pack(2, 2, 3),
            lambda: packed(2), lambda: sent("z")],
        5: [lambda: pass_down(2), lambda: start_down(4), lambda: gate_up(2, 0, 3, 256, 256),
            lambda: gate_up(2, 3, 4)],
        6: [lambda: sent("x"), lambda: sent("m")],
        8: [lambda: pass_down(3)],
        10: [lambda: pass_down(4), start_out],
        13: [lambda: restore(0)],
        14: [pass_out, lambda: sent("w")],
        15: [lambda: restore(1)],
        17: [share_out],
        18: [lambda: restore(2), lambda: project(0)],
        19: [lambda: project(1)],
    }
    units = [(0, 1), (0, 0), (1, 1), (1, 0), (0, 3), (1, 3), (0, 2), (1, 2)]
    units += [(2, 2), (2, 1), (2, 3), (2, 0)]
    units += [(3, 2), (3, 1), (3, 3), (4, 2), (4, 1), (4, 3), (3, 0), (4, 0)]
    count = len(units)
    for i, (c, k) in enumerate(units):
        if all(unit[0] != c for unit in units[:i]):
            first, width = CHUNKS[c]
            got_all(f"w{c}f", W.at[2, 3, first : first + width])
        down(c, k)
        if i >= 1:
            early(*units[i - 1])
        for hook in hooks.get(i, ()):
            hook()
        if i >= 4:
            late(*units[i - 2])
            finish(*units[i - 4])
    early(*units[-1])
    late(*units[-2])
    finish(*units[-4])
    late(*units[-1])
    finish(*units[-3])
    finish(*units[-2])
    restore(3)
    finish(*units[-1])
    restore(4)
    settle()
    sent("")
    assert len(numbers) == COPIES
    with jax.named_scope("home"):
        for copy in homes:
            copy.wait()


def local(
    queries, key_rows, values, sink_logit, out_weight, out_gain, routed_tokens,
    expert_ids, route_weight, routed_gain, expert_gate, expert_up, expert_down,
):
    anywhere = pl.BlockSpec(memory_space=pl.ANY)
    vmem = pl.BlockSpec(memory_space=pltpu.VMEM)
    smem = pl.BlockSpec(memory_space=pltpu.SMEM)
    scratch = [
        pltpu.VMEM((3, 4, 2048, 256), BF16),
        pltpu.VMEM((4, 256, D), BF16),
        pltpu.VMEM((4, 4, 256, D), BF16),
        pltpu.VMEM((4, 512, D), BF16),
        pltpu.VMEM((4, 4, 512, 256), BF16),
        pltpu.VMEM((4, 2, 64, D), BF16),
        pltpu.VMEM((4, 2, 128, D), BF16),
        pltpu.VMEM((3, 128, D), BF16),
        pltpu.VMEM((4, 128, D), BF16),
        pltpu.VMEM((4, 512, 128), F32),
        pltpu.VMEM((4, 4, 256, 128), BF16),
        pltpu.VMEM((4, 128, 512), BF16),
        pltpu.VMEM((4, 512, 128), BF16),
        pltpu.VMEM((2, 4, 4, 16, 128), F32),
        pltpu.VMEM((3, 16, 128), F32),
        pltpu.VMEM((1024, 256), BF16),
        pltpu.VMEM((2, 128, 1024 + 2 * WINDOW), BF16),
        pltpu.VMEM((1024, 256), BF16),
        pltpu.VMEM((4, 256, 256), BF16),
        pltpu.VMEM((1, D), F32),
        pltpu.VMEM((1, D), F32),
        pltpu.SemaphoreType.REGULAR((4,)),
        pltpu.SemaphoreType.DMA((28,)),
        pltpu.SemaphoreType.DMA((SENDS,)),
        pltpu.SemaphoreType.DMA((COPIES,)),
    ]
    return pl.pallas_call(
        kernel,
        out_shape=(
            jax.ShapeDtypeStruct((256, D), BF16),
            jax.ShapeDtypeStruct((512, D), BF16),
        ),
        in_specs=[
            anywhere, anywhere, anywhere, smem, anywhere, anywhere, anywhere, vmem, vmem,
            anywhere, anywhere, anywhere, anywhere,
        ],
        out_specs=(anywhere, anywhere),
        scratch_shapes=scratch,
        compiler_params=pltpu.CompilerParams(
            collective_id=0, has_side_effects=True, vmem_limit_bytes=67043328
        ),
        name="block",
    )(
        queries, key_rows.T, values.T, sink_logit, out_weight, out_gain.reshape(1, D), routed_tokens,
        expert_ids.T, route_weight.T, routed_gain.reshape(1, D), expert_gate.reshape(D, 256),
        expert_up.reshape(D, 256), expert_down.reshape(D, 256),
    )


def solution(mesh):
    placed = (
        P("ep", "tp"), P("ep", "tp"), P("ep", "tp"), P("tp"), P("tp", None), P(),
        P(("ep", "tp"), None), P(("ep", "tp"), None), P(("ep", "tp"), None), P(),
        P("ep", None, "tp"), P("ep", None, "tp"), P("ep", None, "tp"),
    )
    return jax.shard_map(
        local,
        mesh=mesh,
        in_specs=placed,
        out_specs=(P(("ep", "tp"), None), P(("ep", "tp"), None)),
        check_vma=False,
    )
```

time: 416 us -> 172 us (0.41)
  waiting for transfers between devices: 177 us -> 0 us
  Pallas kernels: 0 us -> 167 us
  other arithmetic: 60 us -> 0 us
  matrix products: 57.6 us -> 0 us
  local copies, waits for them, and re-layouts: 58.5 us -> 3.78 us
  starting transfers between devices: 45.7 us -> 0 us
  between operations: 14.1 us -> 0.65 us
    all_to_all x2 -> x0, waiting for transfers between devices: 175 us -> none  [the longest x1 105 us: local(): lax.all_to_all(produced, 'ep', split_axis=0, concat_axis=2, tiled=True)]
    pallas_call x0 -> x1, Pallas kernels: none -> 167 us  [local(): pl.pallas_call(kernel, out_shape=(jax.ShapeDtypeStruct((256, D), BF16), j...]
    dot_general x7 -> x0, matrix products: 57.6 us -> none  [the longest x1 26.2 us: local(): jnp.einsum('ref,edf->red', hidden, down_piece, preferred_element_type=jnp...]
    all_to_all x2 -> x0, starting transfers between devices: 42 us -> none  [the longest x1 33.3 us: local(): lax.all_to_all(produced, 'ep', split_axis=0, concat_axis=2, tiled=True)]
    gather x3 -> x0, local copies, waits for them, and re-layouts: 32 us -> none  [the longest x2 21 us: local(): jnp.take(returned, flat_dest, axis=0).reshape(token_total, TOP, width)]
    reduce_sum x6 -> x0, other arithmetic: 27.2 us -> none  [the longest x1 20 us: local(): jnp.sum(picked_rows.astype(jnp.float32) * route_weight[:, :, None], axis=1)]
    select_n x3 -> x0, other arithmetic: 16.8 us -> none  [the longest x1 16.8 us: local(): jnp.take(normed, slot_token, axis=0, mode='fill', fill_value=0)]
    all_to_all x1 -> x0, local copies, waits for them, and re-layouts: 11.2 us -> none  [local(): lax.all_to_all(produced, 'ep', split_axis=0, concat_axis=2, tiled=True)]
  transfers between devices with their start and end apart: 8 -> 0, of which waited for: 3 -> 0; matrix products, arithmetic and copies ran while one was open for 40% -> 0% of each run, Pallas kernels for 0% -> 0%
where the time goes in v2:
time: 172 us
  Pallas kernels  167 us (97%)
  local copies, waits for them, and re-layouts  3.78 us (2%)
    pallas_call x1, Pallas kernels, local(): pl.pallas_call(kernel, out_shape=(jax.ShapeDtypeStruct((256, D), BF16), j...  167 us
    unnamed x4, local copies, waits for them, and re-layouts  3.78 us

profile of v2, /device:TPU:0, one launch (start us, length us, event | category | flops | bytes accessed | tf_op | source)
XLA Modules:
  0.0 171.9 jit_solution(5862367593843483120)
XLA Ops:
  0.6 167.4 %block.1 = (bf16[256,2048]{1,0:T(8,128)(2,1)}, bf16[512,2048]{1,0:T(8,128)(2,1)}) custom-call(bf16[1024,256]{1,0:T(8,128)(2,1)} %q_in.1, bf16[64,1024]{1,0:T(8,128)(2,1)} %bitcast.12, bf16[64,1024]{1,0:T(8,128)(2,1)} %bitcast.13, f32[4]{0:T(128)} %sink.1, bf16[256,2048]{1,0:T(8,128)(2,1)} %ow_in.1, f32[1,2048]{1,0:T(1,128)} %bitcast.14, ...), custom_call_target="tpu_custom_call" | custom-call | tf_op jit(solution)/shard_map/block/pallas_call | solution.py:587
  168.1 0.0 copy-start
  168.1 2.5 %copy.17 = bf16[256,2048]{1,0:T(8,128)(2,1)} copy(bf16[256,2048]{1,0:T(8,128)(2,1)} %get-tuple-element.4) | data formatting | bytes 2097152
  170.5 0.0 copy-done
  170.5 1.3 copy.18
Async XLA Ops:
  168.1 2.5 %copy-start = (bf16[512,2048]{1,0:T(8,128)(2,1)S(1)}, bf16[512,2048]{1,0:T(8,128)(2,1)}, u32[]{:S(2)}) copy-start(bf16[512,2048]{1,0:T(8,128)(2,1)} %get-tuple-element.5) | copy-start | bytes 6291460

commit v3 on v2

--- a/solution.py
+++ b/solution.py
@@ -350,13 +350,16 @@
     gate_up(1, 0, 3)
     pass_down(0)
     start_down(1)
+    start_down(2)
     gather_pass(2)
     got("d20", "d23", "d21")
     pack(2, 0, 2)
     pack(2, 3, 4)
+    gate_up(2, 0, 3, 0, 256)
     gather_end(3)
-    gate_up(2, 0, 3, 0, 256)
+    gate_up(2, 0, 3, 384, 128)
     pack_all(3)
+    gate_up(3, 0, 3)
     for m in range(2):
         got_all(f"x{m}f", W.at[m, 3])
     gate_up(1, 3, 4)
@@ -499,41 +502,67 @@
                 base = piece * 256
                 homes.append(local(12 + piece, W.at[1, 0, base : base + 256], mix_out.at[:, base : base + 256]))
 
-    hooks = {
-        0: [lambda: gate_up(0, 3, 4), lambda: gather_end(2)],
-        1: [lambda: pass_down(1), lambda: start_down(2), lambda: gate_up(3, 0, 3)],
-        2: [lambda: late(*units[0]), lambda: gate_up(3, 3, 4)],
-        3: [lambda: start_down(3), lambda: late(*units[1]), lambda: got("d22"), lambda: pack(2, 2, 3),
-            lambda: packed(2), lambda: sent("z")],
-        5: [lambda: pass_down(2), lambda: start_down(4), lambda: gate_up(2, 0, 3, 256, 256),
-            lambda: gate_up(2, 3, 4)],
-        6: [lambda: sent("x"), lambda: sent("m")],
-        8: [lambda: pass_down(3)],
-        10: [lambda: pass_down(4), start_out],
-        13: [lambda: restore(0)],
-        14: [pass_out, lambda: sent("w")],
-        15: [lambda: restore(1)],
-        17: [share_out],
-        18: [lambda: restore(2), lambda: project(0)],
-        19: [lambda: project(1)],
-    }
-    units = [(0, 1), (0, 0), (1, 1), (1, 0), (0, 3), (1, 3), (0, 2), (1, 2)]
+    units = [(c, k) for c in range(2) for k in (1, 0, 3, 2)]
     units += [(2, 2), (2, 1), (2, 3), (2, 0)]
     units += [(3, 2), (3, 1), (3, 3), (4, 2), (4, 1), (4, 3), (3, 0), (4, 0)]
-    count = len(units)
-    for i, (c, k) in enumerate(units):
-        if all(unit[0] != c for unit in units[:i]):
+    arrived = set()
+
+    def produce(i):
+        c, k = units[i]
+        if c not in arrived:
+            arrived.add(c)
             first, width = CHUNKS[c]
             got_all(f"w{c}f", W.at[2, 3, first : first + width])
         down(c, k)
-        if i >= 1:
-            early(*units[i - 1])
+
+    produce(0)
+    gate_up(0, 3, 4)
+    gather_end(2)
+    produce(1)
+    pass_down(1)
+    early(*units[0])
+    gate_up(3, 3, 4)
+    early(*units[1])
+    produce(2)
+    got("d22")
+    pack(2, 2, 3)
+    packed(2)
+    gate_up(2, 0, 3, 256, 128)
+    early(*units[2])
+    pass_down(2)
+    start_down(3)
+    start_down(4)
+    gate_up(2, 3, 4)
+    produce(3)
+    late(*units[0])
+    sent("z")
+
+    hooks = {
+        6: [lambda: sent("x"), lambda: sent("m")],
+        9: [lambda: pass_down(3)],
+        10: [lambda: pass_down(4), start_out],
+        13: [lambda: restore(0)],
+        15: [pass_out, lambda: sent("w"), lambda: restore(1)],
+        17: [share_out],
+        18: [lambda: restore(2)],
+        19: [lambda: project(0)],
+    }
+    passed, ended = 1, 0
+    for i in range(4, len(units)):
+        produce(i)
+        early(*units[i - 1])
         for hook in hooks.get(i, ()):
             hook()
-        if i >= 4:
-            late(*units[i - 2])
-            finish(*units[i - 4])
+        lag = 4 if i < 9 else 3 if i < 12 else 2
+        while passed <= i - lag:
+            late(*units[passed])
+            passed += 1
+        while ended <= i - lag - 3:
+            finish(*units[ended])
+            ended += 1
     early(*units[-1])
+    project(1)
+    finish(*units[-5])
     late(*units[-2])
     finish(*units[-4])
     late(*units[-1])

time: 172 us -> 168 us (0.977)
  Pallas kernels: 167 us -> 163 us
    pallas_call x1, Pallas kernels: 167 us -> 163 us  [local(): pl.pallas_call(kernel, out_shape=(jax.ShapeDtypeStruct((256, D), BF16), j...]
where the time goes in v3:
time: 168 us
  Pallas kernels  163 us (97%)
  local copies, waits for them, and re-layouts  3.78 us (2%)
    pallas_call x1, Pallas kernels, local(): pl.pallas_call(kernel, out_shape=(jax.ShapeDtypeStruct((256, D), BF16), j...  163 us
    unnamed x4, local copies, waits for them, and re-layouts  3.78 us

profile of v3, /device:TPU:0, one launch (start us, length us, event | category | flops | bytes accessed | tf_op | source)
XLA Modules:
  0.0 167.5 jit_solution(639675651630064960)
XLA Ops:
  0.6 163.1 %block.1 = (bf16[256,2048]{1,0:T(8,128)(2,1)}, bf16[512,2048]{1,0:T(8,128)(2,1)}) custom-call(bf16[1024,256]{1,0:T(8,128)(2,1)} %q_in.1, bf16[64,1024]{1,0:T(8,128)(2,1)} %bitcast.12, bf16[64,1024]{1,0:T(8,128)(2,1)} %bitcast.13, f32[4]{0:T(128)} %sink.1, bf16[256,2048]{1,0:T(8,128)(2,1)} %ow_in.1, f32[1,2048]{1,0:T(1,128)} %bitcast.14, ...), custom_call_target="tpu_custom_call" | custom-call | tf_op jit(solution)/shard_map/block/pallas_call | solution.py:616
  163.7 0.0 copy-start
  163.7 2.5 %copy.17 = bf16[256,2048]{1,0:T(8,128)(2,1)} copy(bf16[256,2048]{1,0:T(8,128)(2,1)} %get-tuple-element.4) | data formatting | bytes 2097152
  166.2 0.0 copy-done
  166.2 1.3 copy.18
Async XLA Ops:
  163.7 2.5 %copy-start = (bf16[512,2048]{1,0:T(8,128)(2,1)S(1)}, bf16[512,2048]{1,0:T(8,128)(2,1)}, u32[]{:S(2)}) copy-start(bf16[512,2048]{1,0:T(8,128)(2,1)} %get-tuple-element.5) | copy-start | bytes 6291460

commit v4 on v3

--- a/solution.py
+++ b/solution.py
@@ -11,7 +11,7 @@
 WINDOW = 128
 SEQ = 32768
 EPS = 1e-06
-COPIES = 117
+COPIES = 119
 SENDS = 56
 
 
@@ -220,7 +220,11 @@
         copy.wait()
     send("halo_n", KV.at[:, :, 1024 : 1024 + WINDOW], KV.at[:, :, 0:WINDOW], after, "halo")
     send("halo_p", KV.at[:, :, WINDOW : 2 * WINDOW], KV.at[:, :, 1024 + WINDOW :], before, "halo")
-    start_tile(0)
+    for name, j, dev, halves in (("r", 3, yr, (0, 64)), ("l", 1, yl, (64, 0))):
+        for part, row in zip("ab", halves):
+            rows = slice(row, row + 64)
+            send(f"y0{name}{part}", T.at[0, 0, rows], T.at[0, j, rows], dev)
+    send("d00", T.at[0, 0, 0:128], T.at[0, 0, 128:256], sib, "d0")
     start_weight(1, here[3])
     here[5].wait()
     start_down(0)
@@ -322,8 +326,17 @@
     send("myl", MT.at[0, 0], MT.at[0, 1], yl, "my")
     send("myo", MT.at[0, 0], MT.at[0, 2], yo, "my")
     with jax.named_scope("attend"):
-        attend(2, 6)
-    gather_pass(0)
+        attend(2, 4)
+    got("y0ra")
+    send("y0fr", T.at[0, 3, 0:64], T.at[0, 2, 0:64], yr, "y0f")
+    got("y0la")
+    send("y0fl", T.at[0, 1, 64:128], T.at[0, 2, 64:128], yl, "y0f")
+    with jax.named_scope("attend"):
+        attend(4, 6)
+    got("y0rb")
+    send("d03", T.at[0, 3, 0:128], T.at[0, 3, 128:256], sib, "d0")
+    got("y0lb")
+    send("d01", T.at[0, 1, 0:128], T.at[0, 1, 128:256], sib, "d0")
     gather_start(1)
     gather_start(3)
     send_tile(2)
@@ -359,7 +372,13 @@
     gather_end(3)
     gate_up(2, 0, 3, 384, 128)
     pack_all(3)
-    gate_up(3, 0, 3)
+    gate_up(3, 0, 1)
+    gather_end(2)
+    gate_up(3, 1, 3)
+    got("d22")
+    pack(2, 2, 3)
+    packed(2)
+    gate_up(2, 0, 3, 256, 128)
     for m in range(2):
         got_all(f"x{m}f", W.at[m, 3])
     gate_up(1, 3, 4)
@@ -517,17 +536,12 @@
 
     produce(0)
     gate_up(0, 3, 4)
-    gather_end(2)
     produce(1)
     pass_down(1)
     early(*units[0])
     gate_up(3, 3, 4)
     early(*units[1])
     produce(2)
-    got("d22")
-    pack(2, 2, 3)
-    packed(2)
-    gate_up(2, 0, 3, 256, 128)
     early(*units[2])
     pass_down(2)
     start_down(3)

time: 168 us -> 168 us (level)
  no operation moved by 1% of the time
where the time goes in v4:
time: 168 us
  Pallas kernels  163 us (97%)
  local copies, waits for them, and re-layouts  3.78 us (2%)
    pallas_call x1, Pallas kernels, local(): pl.pallas_call(kernel, out_shape=(jax.ShapeDtypeStruct((256, D), BF16), j...  163 us
    unnamed x4, local copies, waits for them, and re-layouts  3.78 us

profile of v4, /device:TPU:0, one launch (start us, length us, event | category | flops | bytes accessed | tf_op | source)
XLA Modules:
  0.0 167.7 jit_solution(10035907640998591792)
XLA Ops:
  0.6 163.3 %block.1 = (bf16[256,2048]{1,0:T(8,128)(2,1)}, bf16[512,2048]{1,0:T(8,128)(2,1)}) custom-call(bf16[1024,256]{1,0:T(8,128)(2,1)} %q_in.1, bf16[64,1024]{1,0:T(8,128)(2,1)} %bitcast.12, bf16[64,1024]{1,0:T(8,128)(2,1)} %bitcast.13, f32[4]{0:T(128)} %sink.1, bf16[256,2048]{1,0:T(8,128)(2,1)} %ow_in.1, f32[1,2048]{1,0:T(1,128)} %bitcast.14, ...), custom_call_target="tpu_custom_call" | custom-call | tf_op jit(solution)/shard_map/block/pallas_call | solution.py:630
  163.9 0.0 copy-start
  163.9 2.5 %copy.17 = bf16[256,2048]{1,0:T(8,128)(2,1)} copy(bf16[256,2048]{1,0:T(8,128)(2,1)} %get-tuple-element.4) | data formatting | bytes 2097152
  166.4 0.0 copy-done
  166.4 1.3 copy.18
Async XLA Ops:
  163.9 2.5 %copy-start = (bf16[512,2048]{1,0:T(8,128)(2,1)S(1)}, bf16[512,2048]{1,0:T(8,128)(2,1)}, u32[]{:S(2)}) copy-start(bf16[512,2048]{1,0:T(8,128)(2,1)} %get-tuple-element.5) | copy-start | bytes 6291460
